TPU v7x, 32 devices: a whole 2x2x4 slice. The times are simulated.
32 devices in a mesh: sp: 4 (over z), dp: 8 (over y, x, core).
Axes of the slice: x: 2, y: 2, z: 4, core: 2. Of those that a mesh axis runs over, the one named last changes fastest.
Arguments:
- value_half: bfloat16 [8, 1536, 2048], P('dp', 'sp'), may hold values from -6 to 6
- gate_half: bfloat16 [8, 1536, 2048], P('dp', 'sp'), may hold values from -9 to 9
- conv_taps: bfloat16 [31, 2048], replicated, may hold values from -1 to 1
- norm_gain: float32 [2048], replicated, may hold values from 0.1 to 1.9
- norm_shift: float32 [2048], replicated, may hold values from -3 to 3
- out_weight: bfloat16 [2048, 2048], P('dp', 'sp'), may hold values from -0.125 to 0.125
Outputs:
- module_out: bfloat16 [8, 1536, 2048], P('dp', 'sp')
All inputs are finite; a program needn't handle non-finite values.
Results may differ from a plain program's by a relative error of at most 0.0064.
Values may be sent and summed in bfloat16 or wider, within the bound.
A program may use at most 64 MiB of HBM per device.

v0:
```python
import jax
import jax.numpy as jnp
from jax import lax
from jax.sharding import PartitionSpec as P

EPSILON = 1e-06


def passed_along(value, axis, steps):
    count = lax.axis_size(axis)
    initial, last = (max(0, -steps), min(count, count - steps))
    return lax.ppermute(value, axis, [(source, source + steps) for source in range(initial, last)])


def causal_mix(padded, conv_taps, length):
    tap_count = conv_taps.shape[0]
    running = jnp.zeros((length, padded.shape[1]), jnp.float32)
    for tap_index in range(tap_count):
        running = running + padded[tap_index : tap_index + length].astype(jnp.float32) * conv_taps[
            tap_index
        ].astype(jnp.float32)
    return running.astype(jnp.bfloat16)


def per_device(value_half, gate_half, conv_taps, norm_gain, norm_shift, out_weight):
    tap_count = conv_taps.shape[0]
    tok_rows = value_half.shape[1]
    gated = (
        value_half[0].astype(jnp.float32) * jax.nn.sigmoid(gate_half[0].astype(jnp.float32))
    ).astype(jnp.bfloat16)
    tail_rows = gated[tok_rows - (tap_count - 1) :]
    history = passed_along(tail_rows, "sp", 1)
    padded = jnp.concatenate([history, gated], 0)
    convolved = causal_mix(padded, conv_taps, tok_rows)
    widened = convolved.astype(jnp.float32)
    mean_row = jnp.mean(widened, axis=-1, keepdims=True)
    centered = widened - mean_row
    variance = jnp.mean(centered * centered, axis=-1, keepdims=True)
    normed = centered * lax.rsqrt(variance + EPSILON) * norm_gain + norm_shift
    activated = jax.nn.silu(normed).astype(jnp.bfloat16)
    row_block = lax.all_gather(out_weight, "sp", axis=1, tiled=True)
    projected = jnp.dot(
        activated,
        lax.all_gather(row_block, "dp", axis=0, tiled=True),
        preferred_element_type=jnp.float32,
    )
    return projected.astype(jnp.bfloat16)[None]


def solution(mesh):
    placed = (P("dp", "sp", None), P("dp", "sp", None), P(), P(), P(), P("dp", "sp"))
    return jax.shard_map(
        per_device, mesh=mesh, in_specs=placed, out_specs=P("dp", "sp", None), check_vma=False
    )
```

profile of v0, /device:TPU:0, one launch (start us, length us, event | category | flops | bytes accessed | tf_op | source)
XLA Modules:
  0.0 110.5 jit_solution(4330929815768049006)
XLA Ops:
  6.5 0.0 copy-start
  6.5 0.0 all-gather.3.cloned.1.call-start
  6.5 0.7 all-gather.3.cloned.1.call-update
  7.3 0.0 all-gather.5.cloned.1.call-start
  7.3 32.3 %all-gather.3.cloned.1.call-done = bf16[256,2048]{1,0:T(8,128)(2,1)} async-done(((bf16[256,512]{1,0:T(8,128)(2,1)}), bf16[256,2048]{1,0:T(8,128)(2,1)}) %all-gather.3.cloned.1.call-update) | async-done | bytes 1048592 | tf_op jit(solution)/shard_map/all_gather | solution.py:41
  39.6 0.0 all-gather.5.cloned.1.call-update
  39.7 2.8 %multiply_convert_fusion = bf16[1,384,2048]{2,1,0:T(8,128)(2,1)S(1)} fusion(bf16[1,384,2048]{2,1,0:T(8,128)(2,1)} %param.6, bf16[1,384,2048]{2,1,0:T(8,128)(2,1)} %param.7), kind=kLoop, calls=%fused_computation.42 | loop fusion | flops 5505024 | bytes 4718592 | tf_op jit(solution)/shard_map/convert_element_type | solution.py:30
  42.5 0.0 copy-start.1
  42.5 0.0 copy-start.2
  42.5 3.4 %collective-permute-start = (bf16[30,2048]{1,0:T(8,128)(2,1)S(1)}, bf16[30,2048]{1,0:T(8,128)(2,1)S(1)}, u32[]{:S(2)}, u32[]{:S(2)}) collective-permute-start(bf16[30,2048]{1,0:T(8,128)(2,1)S(1)} %slice_bitcast_fusion), channel_id=1, source_target_pairs={{0,8},{8,16},{16,24},{1,9},{9,17},{17,25},{2,10},{10,18},{18,26},{... | collective-permute-start | bytes 368648 | tf_op jit(solution)/shard_map/ppermute | solution.py:12
  45.9 0.0 copy-done
  45.9 0.1 slice_convert_fusion.30
  46.0 0.1 slice_convert_fusion.29
  46.1 2.3 %collective-permute-done = bf16[30,2048]{1,0:T(8,128)(2,1)S(1)} collective-permute-done((bf16[30,2048]{1,0:T(8,128)(2,1)S(1)}, bf16[30,2048]{1,0:T(8,128)(2,1)S(1)}, u32[]{:S(2)}, u32[]{:S(2)}) %collective-permute-start) | collective-permute-done | bytes 122912 | tf_op jit(solution)/shard_map/ppermute | solution.py:12
  48.4 14.3 %convert_reduce_fusion = (f32[384]{0:T(512)S(1)}, bf16[384,2048]{1,0:T(8,128)(2,1)S(1)}) fusion(f32[2048]{0:T(1024)S(1)} %bitcast.67, bf16[384,2048]{1,0:T(8,128)(2,1)S(1)} %bitcast.37, f32[2048]{0:T(1024)S(1)} %bitcast.68, bf16[30,2048]{1,0:T(8,128)(2,1)S(1)} %collective-permute-done, f32[2048]{0:T(1024)S(1)} %bitcast.39, f32[2048]{0:T(1024)S(1)} %bitcast.40, ...), kind=kLoop, calls=%fused_computation.30 | loop fusion | flops 145489536 | bytes 3524096 | tf_op jit(solution)/shard_map/reduce_sum | solution.py:36
  62.7 0.6 fusion.2
  63.2 31.9 %all-gather.5.cloned.1.call-done = bf16[2048,2048]{1,0:T(8,128)(2,1)} async-done(((bf16[256,2048]{1,0:T(8,128)(2,1)}), bf16[2048,2048]{1,0:T(8,128)(2,1)}) %all-gather.5.cloned.1.call-update) | async-done | bytes 8388624 | tf_op jit(solution)/shard_map/all_gather | solution.py:44
  95.2 0.0 copy-done.1
  95.2 0.0 copy-done.2
  95.2 8.5 %fusion.11 = bf16[1,384,2048]{2,1,0:T(8,128)(2,1)} fusion(bf16[2048,2048]{1,0:T(8,128)(2,1)} %all-gather.5.cloned.1.call-done, bf16[384,2048]{1,0:T(8,128)(2,1)S(1)} %get-tuple-element.6, f32[2048]{0:T(1024)S(1)} %copy-done.1, f32[2048]{0:T(1024)S(1)} %copy-done.2, f32[384]{0:T(512)S(1)} %add_rsqrt_fusion, f32[384]{0:T(512)S(1)} %broadcast_multiply_fusion), kind=kOutput, calls=%fused_computation.45 | convolution fusion | flops 3229876224 | bytes 11553792 | tf_op jit(solution)/shard_map/dot_general | solution.py:42
  (3 shorter events, 0.0 us)
Async XLA Ops:
  6.5 39.4 %copy-start = (bf16[31,2048]{1,0:T(8,128)(2,1)S(1)}, bf16[31,2048]{1,0:T(8,128)(2,1)}, u32[]{:S(2)}) copy-start(bf16[31,2048]{1,0:T(8,128)(2,1)} %param.8) | copy-start | bytes 380932
  6.5 33.1 %all-gather.3.cloned.1.call-start = ((), (), s32[]{:S(2)}) async-start(), calls=%async_computation | async-start | bytes 1310720 | tf_op jit(solution)/shard_map/all_gather | solution.py:41
  7.3 87.9 %all-gather.5.cloned.1.call-start = ((), (), s32[]{:S(2)}) async-start(), calls=%async_computation.1 | async-start | bytes 9437184 | tf_op jit(solution)/shard_map/all_gather | solution.py:44
  42.5 52.7 %copy-start.1 = (f32[2048]{0:T(1024)S(1)}, f32[2048]{0:T(1024)}, u32[]{:S(2)}) copy-start(f32[2048]{0:T(1024)} %param.10) | copy-start | bytes 24580
  42.5 52.7 %copy-start.2 = (f32[2048]{0:T(1024)S(1)}, f32[2048]{0:T(1024)}, u32[]{:S(2)}) copy-start(f32[2048]{0:T(1024)} %param.9) | copy-start | bytes 24580
  42.5 5.9 %collective-permute-start = (bf16[30,2048]{1,0:T(8,128)(2,1)S(1)}, bf16[30,2048]{1,0:T(8,128)(2,1)S(1)}, u32[]{:S(2)}, u32[]{:S(2)}) collective-permute-start(bf16[30,2048]{1,0:T(8,128)(2,1)S(1)} %slice_bitcast_fusion), channel_id=1, source_target_pairs={{0,8},{8,16},{16,24},{1,9},{9,17},{17,25},{2,10},{10,18},{18,26},{... | collective-permute-start | bytes 368648 | tf_op jit(solution)/shard_map/ppermute | solution.py:12
Sparse Core Ops, SparseCore 0:
  8.9 30.6 all-gather.2
  41.5 53.6 all-gather.4
where the time goes:
time: 111 us
  waiting for transfers between devices  67.3 us (61%)
  other arithmetic  17.8 us (16%)
  between operations  13.5 us (12%)
  matrix products  8.49 us (8%)
  starting transfers between devices  3.4 us (3%)
    all_gather x1, waiting for transfers between devices, per_device(): row_block = lax.all_gather(out_weight, 'sp', axis=1, tiled=True)  32.3 us
    all_gather x1, waiting for transfers between devices, per_device(): lax.all_gather(row_block, 'dp', axis=0, tiled=True)  31.9 us
    reduce_sum x1, other arithmetic, per_device(): mean_row = jnp.mean(widened, axis=-1, keepdims=True)  14.3 us
    dot_general x1, matrix products, per_device(): jnp.dot(activated, lax.all_gather(row_block, 'dp', axis=0, tiled=True), p...  8.49 us
    ppermute x1, starting transfers between devices, passed_along(): lax.ppermute(value, axis, [(source, source + steps) for source in range(i...  3.36 us
    convert_element_type x1, other arithmetic, per_device(): gated = (value_half[0].astype(jnp.float32) * jax.nn.sigmoid(gate_half[0]....  2.79 us
    ppermute x1, waiting for transfers between devices, passed_along(): lax.ppermute(value, axis, [(source, source + steps) for source in range(i...  2.29 us
  transfers between devices with their start and end apart: 3, of which 3 were waited for; matrix products, arithmetic and copies ran while one was open for 16% of the time, Pallas kernels for 0%

commit v1 on v0

--- a/solution.py
+++ b/solution.py
@@ -38,7 +38,12 @@
     variance = jnp.mean(centered * centered, axis=-1, keepdims=True)
     normed = centered * lax.rsqrt(variance + EPSILON) * norm_gain + norm_shift
     activated = jax.nn.silu(normed).astype(jnp.bfloat16)
-    row_block = lax.all_gather(out_weight, "sp", axis=1, tiled=True)
+    ring = [out_weight]
+    for hop in range(3):
+        ring.append(lax.ppermute(ring[-1], "sp", [(dev, (dev + 1) % 4) for dev in range(4)]))
+    row_block = jnp.roll(
+        jnp.concatenate(ring[::-1], axis=1), (lax.axis_index("sp") + 1) * ring[0].shape[1], axis=1
+    )
     projected = jnp.dot(
         activated,
         lax.all_gather(row_block, "dp", axis=0, tiled=True),

time: 111 us -> 111 us (level)
  local copies, waits for them, and re-layouts: 0.05 us -> 6.63 us
  waiting for transfers between devices: 67.3 us -> 61.3 us
  other arithmetic: 17.8 us -> 15.9 us
    all_gather x1 -> x0, waiting for transfers between devices: 32.3 us -> none  [per_device(): row_block = lax.all_gather(out_weight, 'sp', axis=1, tiled=True)]
    ppermute x0 -> x3, waiting for transfers between devices: none -> 26.3 us  [per_device(): lax.ppermute(ring[-1], 'sp', [(dev, (dev + 1) % 4) for dev in range(4)])]
    unnamed x6 -> x27, local copies, waits for them, and re-layouts: 0.02 us -> 5.53 us
    ppermute x0 -> x3, starting transfers between devices: none -> 3.06 us  [per_device(): lax.ppermute(ring[-1], 'sp', [(dev, (dev + 1) % 4) for dev in range(4)])]
    ppermute x1, starting transfers between devices: 3.36 us -> 1.3 us  [passed_along(): lax.ppermute(value, axis, [(source, source + steps) for source in range(i...]
    convert_element_type x1, other arithmetic: 2.79 us -> 0.86 us  [per_device(): gated = (value_half[0].astype(jnp.float32) * jax.nn.sigmoid(gate_half[0]....]
  transfers between devices with their start and end apart: 3 -> 5, of which waited for: 3 -> 5; matrix products, arithmetic and copies ran while one was open for 16% -> 14% of each run, Pallas kernels for 0% -> 0%
where the time goes in v1:
time: 111 us; the launch traced here: 110 us
  waiting for transfers between devices  61.3 us (55%)
  other arithmetic  15.9 us (14%)
  between operations  13.6 us (12%)
  matrix products  8.5 us (8%)
  local copies, waits for them, and re-layouts  6.63 us (6%)
  starting transfers between devices  4.36 us (4%)
    all_gather x1, waiting for transfers between devices, per_device(): lax.all_gather(row_block, 'dp', axis=0, tiled=True)  32.7 us
    ppermute x3, waiting for transfers between devices, per_device(): lax.ppermute(ring[-1], 'sp', [(dev, (dev + 1) % 4) for dev in range(4)])  26.3 us
    reduce_sum x1, other arithmetic, per_device(): mean_row = jnp.mean(widened, axis=-1, keepdims=True)  14.3 us
    dot_general x1, matrix products, per_device(): jnp.dot(activated, lax.all_gather(row_block, 'dp', axis=0, tiled=True), p...  8.5 us
    unnamed x27, local copies, waits for them, and re-layouts  5.53 us
    ppermute x3, starting transfers between devices, per_device(): lax.ppermute(ring[-1], 'sp', [(dev, (dev + 1) % 4) for dev in range(4)])  3.06 us
    ppermute x1, waiting for transfers between devices, passed_along(): lax.ppermute(value, axis, [(source, source + steps) for source in range(i...  2.29 us
  transfers between devices with their start and end apart: 5, of which 5 were waited for; matrix products, arithmetic and copies ran while one was open for 14% of the time, Pallas kernels for 0%

profile of v1, /device:TPU:0, one launch (start us, length us, event | category | flops | bytes accessed | tf_op | source)
XLA Modules:
  0.0 110.3 jit_solution(1112039941945536667)
XLA Ops:
  6.5 0.0 copy-start.2
  6.5 0.0 all-gather.2.cloned.1.call-start
  6.5 3.1 %collective-permute-start.1 = (bf16[256,512]{1,0:T(8,128)(2,1)}, bf16[256,512]{1,0:T(8,128)(2,1)S(1)}, u32[]{:S(2)}, u32[]{:S(2)}) collective-permute-start(bf16[256,512]{1,0:T(8,128)(2,1)} %param.11), channel_id=1, source_target_pairs={{0,8},{8,16},{16,24},{24,0},{1,9},{9,17},{17,25},{25,1},{2,10},{10... | collective-permute-start | bytes 786440 | tf_op jit(solution)/shard_map/ppermute | solution.py:43
  9.6 8.6 %collective-permute-done.1 = bf16[256,512]{1,0:T(8,128)(2,1)S(1)} collective-permute-done((bf16[256,512]{1,0:T(8,128)(2,1)}, bf16[256,512]{1,0:T(8,128)(2,1)S(1)}, u32[]{:S(2)}, u32[]{:S(2)}) %collective-permute-start.1) | collective-permute-done | bytes 262176 | tf_op jit(solution)/shard_map/ppermute | solution.py:43
  18.2 0.0 copy-start.3
  18.2 0.7 copy-done.3
  18.9 0.0 collective-permute-start.2
  18.9 9.3 %collective-permute-done.2 = bf16[256,512]{1,0:T(8,128)(2,1)S(1)} collective-permute-done((bf16[256,512]{1,0:T(8,128)(2,1)S(1)}, bf16[256,512]{1,0:T(8,128)(2,1)S(1)}, u32[]{:S(2)}, u32[]{:S(2)}) %collective-permute-start.2) | collective-permute-done | bytes 262176 | tf_op jit(solution)/shard_map/ppermute | solution.py:43
  28.2 0.0 copy-start.5
  28.2 0.0 collective-permute-start.3
  28.2 0.0 copy-start.4
  28.2 8.4 %collective-permute-done.3 = bf16[256,512]{1,0:T(8,128)(2,1)S(1)} collective-permute-done((bf16[256,512]{1,0:T(8,128)(2,1)S(1)}, bf16[256,512]{1,0:T(8,128)(2,1)S(1)}, u32[]{:S(2)}, u32[]{:S(2)}) %collective-permute-start.3) | collective-permute-done | bytes 262176 | tf_op jit(solution)/shard_map/ppermute | solution.py:43
  36.6 0.0 copy-start.6
  36.6 0.0 copy-done.5
  36.6 0.7 copy-done.6
  37.3 0.0 copy-start
  37.3 0.0 copy-start.1
  37.3 1.1 %constant_dynamic-update-slice_fusion.5 = bf16[256,4096]{1,0:T(8,128)(2,1)S(1)} fusion(bf16[256,4096]{1,0:T(8,128)(2,1)S(1)} %constant_dynamic-update-slice_fusion.6, bf16[256,512]{1,0:T(8,128)(2,1)} %copy-done.3), kind=kLoop, calls=%fused_computation.93 | loop fusion | bytes 524288
  38.5 1.0 constant_dynamic-update-slice_fusion.4
  39.5 1.0 constant_dynamic-update-slice_fusion.3
  40.4 1.0 constant_dynamic-update-slice_fusion.2
  41.4 0.0 copy-done.4
  41.5 0.0 copy-done.2
  41.5 1.0 constant_dynamic-slice_fusion
  42.6 0.0 copy-start.7
  42.6 0.0 all-gather.2.cloned.1.call-update
  42.6 0.0 copy-done
  42.6 0.0 copy-done.1
  42.6 0.9 multiply_convert_fusion
  43.5 0.0 copy-start.8
  43.5 0.0 copy-start.9
  43.5 1.3 %collective-permute-start = (bf16[30,2048]{1,0:T(8,128)(2,1)S(1)}, bf16[30,2048]{1,0:T(8,128)(2,1)S(1)}, u32[]{:S(2)}, u32[]{:S(2)}) collective-permute-start(bf16[30,2048]{1,0:T(8,128)(2,1)S(1)} %slice_bitcast_fusion), channel_id=1, source_target_pairs={{0,8},{8,16},{16,24},{1,9},{9,17},{17,25},{2,10},{10,18},{18,26},{... | collective-permute-start | bytes 368648 | tf_op jit(solution)/shard_map/ppermute | solution.py:12
  44.8 0.0 copy-done.7
  44.9 0.1 slice_convert_fusion.30
  45.0 0.1 slice_convert_fusion.29
  45.1 2.3 %collective-permute-done = bf16[30,2048]{1,0:T(8,128)(2,1)S(1)} collective-permute-done((bf16[30,2048]{1,0:T(8,128)(2,1)S(1)}, bf16[30,2048]{1,0:T(8,128)(2,1)S(1)}, u32[]{:S(2)}, u32[]{:S(2)}) %collective-permute-start) | collective-permute-done | bytes 122912 | tf_op jit(solution)/shard_map/ppermute | solution.py:12
  47.3 14.3 %convert_reduce_fusion = (f32[384]{0:T(512)S(1)}, bf16[384,2048]{1,0:T(8,128)(2,1)S(1)}) fusion(f32[2048]{0:T(1024)S(1)} %bitcast.67, bf16[384,2048]{1,0:T(8,128)(2,1)S(1)} %bitcast.37, f32[2048]{0:T(1024)S(1)} %bitcast.68, bf16[30,2048]{1,0:T(8,128)(2,1)S(1)} %collective-permute-done, f32[2048]{0:T(1024)S(1)} %bitcast.39, f32[2048]{0:T(1024)S(1)} %bitcast.40, ...), kind=kLoop, calls=%fused_computation.30 | loop fusion | flops 145489536 | bytes 3524096 | tf_op jit(solution)/shard_map/reduce_sum | solution.py:36
  61.6 0.6 fusion.2
  62.2 32.7 %all-gather.2.cloned.1.call-done = bf16[2048,2048]{1,0:T(8,128)(2,1)} async-done(((bf16[256,2048]{1,0:T(8,128)(2,1)}), bf16[2048,2048]{1,0:T(8,128)(2,1)}) %all-gather.2.cloned.1.call-update) | async-done | bytes 8388624 | tf_op jit(solution)/shard_map/all_gather | solution.py:49
  94.9 0.0 copy-done.8
  94.9 0.0 copy-done.9
  94.9 8.5 %fusion.11 = bf16[1,384,2048]{2,1,0:T(8,128)(2,1)} fusion(bf16[2048,2048]{1,0:T(8,128)(2,1)} %all-gather.2.cloned.1.call-done, bf16[384,2048]{1,0:T(8,128)(2,1)S(1)} %get-tuple-element.6, f32[2048]{0:T(1024)S(1)} %copy-done.8, f32[2048]{0:T(1024)S(1)} %copy-done.9, f32[384]{0:T(512)S(1)} %add_rsqrt_fusion, f32[384]{0:T(512)S(1)} %broadcast_multiply_fusion), kind=kOutput, calls=%fused_computation.45 | convolution fusion | flops 3229876224 | bytes 11553792 | tf_op jit(solution)/shard_map/dot_general | solution.py:47
  (7 shorter events, 0.1 us)
Async XLA Ops:
  6.5 34.9 %copy-start.2 = (bf16[256,512]{1,0:T(8,128)(2,1)S(1)}, bf16[256,512]{1,0:T(8,128)(2,1)}, u32[]{:S(2)}) copy-start(bf16[256,512]{1,0:T(8,128)(2,1)} %param.11) | copy-start | bytes 786436
  6.5 88.4 %all-gather.2.cloned.1.call-start = ((), (), s32[]{:S(2)}) async-start(), calls=%async_computation | async-start | bytes 9437184 | tf_op jit(solution)/shard_map/all_gather | solution.py:49
  6.5 11.7 %collective-permute-start.1 = (bf16[256,512]{1,0:T(8,128)(2,1)}, bf16[256,512]{1,0:T(8,128)(2,1)S(1)}, u32[]{:S(2)}, u32[]{:S(2)}) collective-permute-start(bf16[256,512]{1,0:T(8,128)(2,1)} %param.11), channel_id=1, source_target_pairs={{0,8},{8,16},{16,24},{24,0},{1,9},{9,17},{17,25},{25,1},{2,10},{10... | collective-permute-start | bytes 786440 | tf_op jit(solution)/shard_map/ppermute | solution.py:43
  18.2 0.7 copy-start.3
  18.9 9.3 %collective-permute-start.2 = (bf16[256,512]{1,0:T(8,128)(2,1)S(1)}, bf16[256,512]{1,0:T(8,128)(2,1)S(1)}, u32[]{:S(2)}, u32[]{:S(2)}) collective-permute-start(bf16[256,512]{1,0:T(8,128)(2,1)S(1)} %collective-permute-done.1), channel_id=1, source_target_pairs={{0,8},{8,16},{16,24},{24,0},{1,9},{9,17},{17,25},{25,1},{2,10},{10... | collective-permute-start | bytes 786440 | tf_op jit(solution)/shard_map/ppermute | solution.py:43
  28.2 8.4 %copy-start.5 = (bf16[256,512]{1,0:T(8,128)(2,1)}, bf16[256,512]{1,0:T(8,128)(2,1)S(1)}, u32[]{:S(2)}) copy-start(bf16[256,512]{1,0:T(8,128)(2,1)S(1)} %collective-permute-done.2) | copy-start | bytes 786436
  28.2 8.4 %collective-permute-start.3 = (bf16[256,512]{1,0:T(8,128)(2,1)S(1)}, bf16[256,512]{1,0:T(8,128)(2,1)S(1)}, u32[]{:S(2)}, u32[]{:S(2)}) collective-permute-start(bf16[256,512]{1,0:T(8,128)(2,1)S(1)} %collective-permute-done.2), channel_id=1, source_target_pairs={{0,8},{8,16},{16,24},{24,0},{1,9},{9,17},{17,25},{25,1},{2,10},{10... | collective-permute-start | bytes 786440 | tf_op jit(solution)/shard_map/ppermute | solution.py:43
  28.2 13.3 %copy-start.4 = (bf16[256,512]{1,0:T(8,128)(2,1)S(1)}, bf16[256,512]{1,0:T(8,128)(2,1)}, u32[]{:S(2)}) copy-start(bf16[256,512]{1,0:T(8,128)(2,1)} %copy-done.3) | copy-start | bytes 786436
  36.6 0.7 copy-start.6
  37.3 5.3 %copy-start = (bf16[1,384,2048]{2,1,0:T(8,128)(2,1)S(1)}, bf16[1,384,2048]{2,1,0:T(8,128)(2,1)}, u32[]{:S(2)}) copy-start(bf16[1,384,2048]{2,1,0:T(8,128)(2,1)} %param.6) | copy-start | bytes 4718596
  37.3 5.3 %copy-start.1 = (bf16[1,384,2048]{2,1,0:T(8,128)(2,1)S(1)}, bf16[1,384,2048]{2,1,0:T(8,128)(2,1)}, u32[]{:S(2)}) copy-start(bf16[1,384,2048]{2,1,0:T(8,128)(2,1)} %param.7) | copy-start | bytes 4718596
  42.6 2.3 %copy-start.7 = (bf16[31,2048]{1,0:T(8,128)(2,1)S(1)}, bf16[31,2048]{1,0:T(8,128)(2,1)}, u32[]{:S(2)}) copy-start(bf16[31,2048]{1,0:T(8,128)(2,1)} %param.8) | copy-start | bytes 380932
  43.5 51.4 %copy-start.8 = (f32[2048]{0:T(1024)S(1)}, f32[2048]{0:T(1024)}, u32[]{:S(2)}) copy-start(f32[2048]{0:T(1024)} %param.10) | copy-start | bytes 24580
  43.5 51.4 %copy-start.9 = (f32[2048]{0:T(1024)S(1)}, f32[2048]{0:T(1024)}, u32[]{:S(2)}) copy-start(f32[2048]{0:T(1024)} %param.9) | copy-start | bytes 24580
  43.5 3.8 %collective-permute-start = (bf16[30,2048]{1,0:T(8,128)(2,1)S(1)}, bf16[30,2048]{1,0:T(8,128)(2,1)S(1)}, u32[]{:S(2)}, u32[]{:S(2)}) collective-permute-start(bf16[30,2048]{1,0:T(8,128)(2,1)S(1)} %slice_bitcast_fusion), channel_id=1, source_target_pairs={{0,8},{8,16},{16,24},{1,9},{9,17},{17,25},{2,10},{10,18},{18,26},{... | collective-permute-start | bytes 368648 | tf_op jit(solution)/shard_map/ppermute | solution.py:12
Sparse Core Ops, SparseCore 0:
  42.7 52.1 all-gather.1
